TPU v7x, 32 devices: a whole 2x2x4 slice. The times are simulated.
32 devices in a mesh: dp: 4 (over y, x), kv: 4 (over z), tp: 2 (over core).
Axes of the slice: x: 2, y: 2, z: 4, core: 2. Of those that a mesh axis runs over, the one named last changes fastest.
Arguments:
- tokens: bfloat16 [32, 2048], P('dp', 'kv'), may hold values from -6 to 6
- pre_gain: float32 [2048], P('kv'), may hold values from 0.1 to 1.9
- query_weight: bfloat16 [2048, 1024], P('kv', 'tp'), may hold values from -0.125 to 0.125
- key_weight: bfloat16 [2048, 1024], P('kv', 'tp'), may hold values from -0.125 to 0.125
- value_weight: bfloat16 [2048, 1024], P('kv', 'tp'), may hold values from -0.125 to 0.125
- outgate_weight: bfloat16 [2048, 1024], P('kv', 'tp'), may hold values from -0.125 to 0.125
- input_gate_weight: bfloat16 [2048, 4], replicated, may hold values from -0.125 to 0.125
- forget_gate_weight: bfloat16 [2048, 4], replicated, may hold values from -0.125 to 0.125
- cache_keys: bfloat16 [32, 64, 1024], P(('dp', 'kv'), None, 'tp'), may hold values from -6 to 6
- cache_values: bfloat16 [32, 64, 1024], P(('dp', 'kv'), None, 'tp'), may hold values from -6 to 6
- cache_input: float32 [32, 64, 4], P(('dp', 'kv'), None, 'tp'), may hold values from -6 to 250
- cache_forget: float32 [32, 64, 4], P(('dp', 'kv'), None, 'tp'), may hold values from -0.7 to 0
- lengths: int32 [32], P(('dp', 'kv')), may hold values from 1 to 64, 819 in all
- state_matrix: float32 [32, 4, 256, 256], P(('dp', 'kv'), 'tp'), may hold values from -6 to 6
- state_norm: float32 [32, 4, 256], P(('dp', 'kv'), 'tp'), may hold values from -6 to 6
- state_max: float32 [32, 4], P(('dp', 'kv'), 'tp'), may hold values from -4 to 253
- head_gain: float32 [1024], P('tp'), may hold values from 0.1 to 1.9
- out_weight: bfloat16 [1024, 2048], P('tp', 'kv'), may hold values from -0.375 to 0.375
- mixer_gain: float32 [2048], replicated, may hold values from 0.1 to 1.9
- gate_weight: bfloat16 [2048, 5632], P(None, ('kv', 'tp')), may hold values from -0.125 to 0.125
- up_weight: bfloat16 [2048, 5632], P(None, ('kv', 'tp')), may hold values from -0.125 to 0.125
- down_weight: bfloat16 [5632, 2048], P(('kv', 'tp')), may hold values from -0.21875 to 0.21875
Outputs:
- layer_out: bfloat16 [32, 2048], P('dp', ('kv', 'tp'))
Inputs may be any that keep to these rules, and one draw needn't show every extreme that they name: `lengths`: positions from a sequence's length on take no part.
All inputs are finite; a program needn't handle non-finite values. No bound on the sum of `lengths` on one device may be relied on, other than what follows from the above.
Results may differ from a plain program's by a relative error of at most 0.018.
Values may be sent and summed in bfloat16 or wider, within the bound.
No kernel may reach another device: no remote copies, remote signals or barrier semaphores. Data moves between devices by JAX's collectives and lax.ppermute only.
A program may use at most 64 MiB of HBM per device.

v0:
```python
import jax
import jax.numpy as jnp
from jax import lax
from jax.sharding import PartitionSpec as P

EPS = 1e-06


def per_device(
    tokens,
    pre_gain,
    query_weight,
    key_weight,
    value_weight,
    outgate_weight,
    input_gate_weight,
    forget_gate_weight,
    cache_keys,
    cache_values,
    cache_input,
    cache_forget,
    lengths,
    state_matrix,
    state_norm,
    state_max,
    head_gain,
    out_weight,
    mixer_gain,
    gate_weight,
    up_weight,
    down_weight,
):
    col_width = tokens.shape[1]
    own_seqs = cache_keys.shape[0]
    block_len = cache_keys.shape[1]
    head_count = state_max.shape[1]
    head_size = state_norm.shape[2]
    shard_index = lax.axis_index("kv")
    half_index = lax.axis_index("tp")
    kv_count = lax.axis_size("kv")
    model_width = col_width * kv_count
    token_values = tokens.astype(jnp.float32)
    squares = jnp.sum(token_values * token_values, axis=1)
    normed = (token_values * pre_gain[None, :]).astype(jnp.bfloat16)
    corner = (shard_index * col_width, half_index * head_count)
    gate_pair = jnp.concatenate(
        [
            lax.dynamic_slice(input_gate_weight, corner, (col_width, head_count)),
            lax.dynamic_slice(forget_gate_weight, corner, (col_width, head_count)),
        ],
        axis=1,
    )

    def product(weight):
        return jnp.dot(normed, weight, preferred_element_type=jnp.float32)

    query_term = product(query_weight)
    key_term = product(key_weight)
    value_term = product(value_weight)
    outgate_term = product(outgate_weight)
    gate_term = product(gate_pair)
    square_totals = lax.psum(squares, "kv")
    query_sum, key_sum, value_sum, outgate_sum, gate_sum = (
        lax.psum_scatter(query_term, "kv", scatter_dimension=0, tiled=True),
        lax.psum_scatter(key_term, "kv", scatter_dimension=0, tiled=True),
        lax.psum_scatter(value_term, "kv", scatter_dimension=0, tiled=True),
        lax.psum_scatter(outgate_term, "kv", scatter_dimension=0, tiled=True),
        lax.psum_scatter(gate_term, "kv", scatter_dimension=0, tiled=True),
    )
    own_squares = lax.dynamic_slice_in_dim(square_totals, shard_index * own_seqs, own_seqs, 0)
    scale_first = lax.rsqrt(own_squares / model_width + EPS)[:, None]
    query = (scale_first * query_sum).astype(jnp.bfloat16)
    keys_new = (scale_first * key_sum).astype(jnp.bfloat16)
    values_new = (scale_first * value_sum).astype(jnp.bfloat16)
    outgate = (scale_first * outgate_sum).astype(jnp.bfloat16)
    gate_values = scale_first * gate_sum
    in_gate = gate_values[:, :head_count]
    forget_new = jax.nn.log_sigmoid(gate_values[:, head_count:])
    query_heads = query.reshape(own_seqs, head_count, head_size)
    key_heads = keys_new.reshape(own_seqs, head_count, head_size)
    value_heads = values_new.reshape(own_seqs, head_count, head_size)
    cached_keys = cache_keys.reshape(own_seqs, block_len, head_count, head_size)
    cached_values = cache_values.reshape(own_seqs, block_len, head_count, head_size)
    inv_root = head_size ** (-0.5)
    live_mask = (lax.broadcasted_iota(jnp.int32, (own_seqs, block_len), 1) < lengths[:, None])[
        :, :, None
    ]
    forget_live = jnp.where(live_mask, cache_forget, jnp.float32(0.0))
    running = jnp.cumsum(forget_live, axis=1)
    total_log = running[:, -1, :] + forget_new
    weight_log = jnp.where(live_mask, total_log[:, None, :] - running + cache_input, -jnp.inf)
    state_log = total_log + state_max
    peak_log = jnp.maximum(jnp.maximum(state_log, in_gate), jnp.max(weight_log, axis=1))
    key_dots = (
        jnp.einsum("shd,slhd->slh", query_heads, cached_keys, preferred_element_type=jnp.float32)
        * inv_root
    )
    block_scores = jnp.exp(weight_log - peak_log[:, None, :]) * key_dots
    query_scaled = query_heads.astype(jnp.float32) * inv_root
    self_score = jnp.exp(in_gate - peak_log) * jnp.sum(
        query_scaled * key_heads.astype(jnp.float32), axis=2
    )
    carried = jnp.exp(state_log - peak_log)
    block_weights = block_scores.astype(jnp.bfloat16)
    memory_read = jnp.einsum(
        "shvd,shd->shv", state_matrix, query_scaled, precision=lax.Precision.HIGHEST
    )
    norm_read = jnp.einsum("shd,shd->sh", state_norm, query_scaled, precision=lax.Precision.HIGHEST)
    numerator = (
        carried[:, :, None] * memory_read
        + jnp.einsum(
            "slh,slhd->shd", block_weights, cached_values, preferred_element_type=jnp.float32
        )
        + self_score[:, :, None] * value_heads.astype(jnp.float32)
    )
    denominator = carried * norm_read + jnp.sum(block_scores, axis=1) + self_score
    hidden = numerator / jnp.maximum(jnp.abs(denominator), 1.0)[:, :, None]
    mixed_heads = (
        hidden.reshape(own_seqs, head_count * head_size)
        * head_gain[None, :]
        * jax.nn.sigmoid(outgate.astype(jnp.float32))
    ).astype(jnp.bfloat16)
    mix_terms = jnp.dot(
        lax.all_gather(mixed_heads, "kv", axis=0, tiled=True),
        out_weight,
        preferred_element_type=jnp.float32,
    )
    mix_sum = lax.psum_scatter(
        mix_terms.astype(jnp.bfloat16), "tp", scatter_dimension=1, tiled=True
    ).astype(jnp.float32)
    narrow = mix_sum.shape[1]
    residual = (
        lax.dynamic_slice_in_dim(token_values, half_index * narrow, narrow, 1) + mix_sum
    ).astype(jnp.bfloat16)
    piece_wide = lax.all_gather(residual, ("kv", "tp"), axis=1, tiled=True).astype(jnp.float32)
    normed_piece = (piece_wide * mixer_gain[None, :]).astype(jnp.bfloat16)
    gate_acc = jnp.dot(normed_piece, gate_weight, preferred_element_type=jnp.float32)
    up_acc = jnp.dot(normed_piece, up_weight, preferred_element_type=jnp.float32)
    sum_squares = jnp.sum(piece_wide * piece_wide, axis=1)
    gate_acc, up_acc, sum_squares = (gate_acc, up_acc, sum_squares)
    scale_mid = lax.rsqrt(sum_squares / model_width + EPS)[:, None]
    hidden_units = (jax.nn.silu(scale_mid * gate_acc) * (scale_mid * up_acc)).astype(jnp.bfloat16)
    summed = lax.psum_scatter(
        lax.dot_general(
            down_weight, hidden_units, (((0,), (1,)), ((), ())), preferred_element_type=jnp.float32
        ),
        ("kv", "tp"),
        scatter_dimension=0,
        tiled=True,
    )
    mixer_out = summed.T
    return (residual.astype(jnp.float32) + mixer_out).astype(jnp.bfloat16)


def solution(mesh):
    in_specs = (
        P("dp", "kv"),
        P("kv"),
        P("kv", "tp"),
        P("kv", "tp"),
        P("kv", "tp"),
        P("kv", "tp"),
        P(),
        P(),
        P(("dp", "kv"), None, "tp"),
        P(("dp", "kv"), None, "tp"),
        P(("dp", "kv"), None, "tp"),
        P(("dp", "kv"), None, "tp"),
        P(("dp", "kv")),
        P(("dp", "kv"), "tp", None, None),
        P(("dp", "kv"), "tp", None),
        P(("dp", "kv"), "tp"),
        P("tp"),
        P("tp", "kv"),
        P(),
        P(None, ("kv", "tp")),
        P(None, ("kv", "tp")),
        P(("kv", "tp"), None),
    )
    out_specs = P("dp", ("kv", "tp"))
    return jax.shard_map(
        per_device, mesh=mesh, in_specs=in_specs, out_specs=out_specs, check_vma=False
    )
```

profile of v0, /device:TPU:0, one launch (start us, length us, event | category | flops | bytes accessed | tf_op | source)
XLA Modules:
  0.0 147.6 jit_solution(3637259032463186697)
XLA Ops:
  6.6 1.6 %multiply_reduce_fusion = f32[8]{0:T(128)} fusion(bf16[8,512]{1,0:T(8,128)(2,1)} %param.22), kind=kLoop, calls=%fused_computation.22 | loop fusion | flops 12280 | bytes 8224 | tf_op jit(solution)/shard_map/reduce_sum | solution.py:43
  8.2 1.9 %fusion.43 = f32[8,512]{1,0:T(8,128)} fusion(bf16[512,512]{1,0:T(8,128)(2,1)} %param.27, f32[512]{0:T(512)} %param.23, bf16[8,512]{1,0:T(8,128)(2,1)} %param.22), kind=kOutput, calls=%fused_computation.73 | convolution fusion | flops 4206592 | bytes 550912 | tf_op jit(solution)/shard_map/dot_general | solution.py:55
  10.0 1.9 %fusion.44 = f32[8,512]{1,0:T(8,128)} fusion(bf16[512,512]{1,0:T(8,128)(2,1)} %param.26, f32[512]{0:T(512)} %param.23, bf16[8,512]{1,0:T(8,128)(2,1)} %param.22), kind=kOutput, calls=%fused_computation.74 | convolution fusion | flops 4206592 | bytes 550912 | tf_op jit(solution)/shard_map/dot_general | solution.py:55
  11.9 1.9 %fusion.46 = f32[8,512]{1,0:T(8,128)} fusion(bf16[512,512]{1,0:T(8,128)(2,1)} %param.24, f32[512]{0:T(512)} %param.23, bf16[8,512]{1,0:T(8,128)(2,1)} %param.22), kind=kOutput, calls=%fused_computation.76 | convolution fusion | flops 4206592 | bytes 550912 | tf_op jit(solution)/shard_map/dot_general | solution.py:55
  15.3 1.9 %fusion.45 = f32[8,512]{1,0:T(8,128)} fusion(bf16[512,512]{1,0:T(8,128)(2,1)} %param.25, f32[512]{0:T(512)} %param.23, bf16[8,512]{1,0:T(8,128)(2,1)} %param.22), kind=kOutput, calls=%fused_computation.75 | convolution fusion | flops 4206592 | bytes 550912 | tf_op jit(solution)/shard_map/dot_general | solution.py:55
  17.1 1.4 fusion.21
  20.3 1.3 dynamic-slice
  22.3 34.1 %all-reduce.8.cloned.1.call-done = (f32[8,512]{1,0:T(8,128)}, f32[8]{0:T(128)}, f32[8,512]{1,0:T(8,128)}, f32[8,512]{1,0:T(8,128)}, f32[8,4]{1,0:T(8,128)}, /*index=5*/f32[8,512]{1,0:T(8,128)}) async-done(((f32[8,512]{1,0:T(8,128)}, f32[8]{0:T(128)}, f32[8,512]{1,0:T(8,128)}, f32[8,512]{1,0:T(8,128)}, f32[8,4]{1,0:T(8,128)}, /*index=5*/f32[8,512]{1,0:T(8,128)}), (f32[8,512]{1,0:T(8,128)}, f32[8]{0:T(128)}, ...) | async-done | bytes 65712
  57.1 0.8 fusion.37
  58.7 1.0 fusion.5
  59.8 0.9 fusion.49
  61.4 0.8 fusion.50
  62.2 1.0 fusion.2
  63.2 0.8 multiply_reduce_fusion.1
  64.0 2.2 %fusion.31 = f32[2,2,1,256]{3,2,1,0:T(1,128)S(1)} fusion(f32[2,2,256,256]{3,2,1,0:T(8,128)} %param.35, f32[2,2,256,1]{2,1,0,3:T(2,128)S(1)} %get-tuple-element.20), kind=kOutput, calls=%fused_computation.46 | convolution fusion | flops 3145728 | bytes 1056768 | tf_op jit(solution)/shard_map/shvd,shd->shv/dot_general | solution.py:105
  66.3 0.8 fusion.39
  67.1 12.0 %all-gather = bf16[4,2,512]{2,1,0:T(2,128)(2,1)S(1)} all-gather(bf16[1,2,512]{2,1,0:T(2,128)(2,1)S(1)} %fusion.39), channel_id=1, replica_groups=mesh['dp'=4,'kv'=4,'tp'=2] {'kv'}, dimensions={0}, use_global_device_ids=true | all-gather | bytes 10240 | tf_op jit(solution)/shard_map/all_gather | solution.py:124
  79.1 0.8 convolution_convert_fusion
  80.0 6.4 %reduce-scatter.3.cloned.1.call-done = bf16[8,256]{1,0:T(8,128)(2,1)} async-done(((bf16[8,512]{1,0:T(8,128)(2,1)}), bf16[8,256]{1,0:T(8,128)(2,1)}) %reduce-scatter.3.cloned.1.call-update) | async-done | bytes 4112 | tf_op jit(solution)/shard_map/reduce_scatter | solution.py:128
  87.0 14.3 %all_gather.7 = bf16[8,2048]{1,0:T(8,128)(2,1)S(1)} all-gather(bf16[8,256]{1,0:T(8,128)(2,1)S(1)} %add_convert_fusion), channel_id=1, replica_groups=mesh['dp'=4,'kv'=4,'tp'=2] {'kv','tp'}, dimensions={1}, use_global_device_ids=true | all-gather | bytes 36864 | tf_op jit(solution)/shard_map/all_gather | solution.py:135
  101.5 2.7 %convolution_multiply_fusion.1 = f32[8,704]{1,0:T(8,128)S(1)} fusion(bf16[2048,704]{0,1:T(8,128)(2,1)} %param.41, bf16[8,2048]{1,0:T(8,128)(2,1)S(1)} %all_gather.7, f32[2048]{0:T(1024)S(1)} %copy-done.3, f32[8]{0:T(128)S(1)} %add_rsqrt_fusion), kind=kOutput, calls=%fused_computation.3 | convolution fusion | flops 23123456 | bytes 2947104 | tf_op jit(solution)/shard_map/dot_general | solution.py:137
  104.2 4.1 %convolution_bitcast_fusion = f32[2048,8]{0,1:T(8,128)} fusion(bf16[704,2048]{1,0:T(8,128)(2,1)S(1)} %copy-done, bf16[2048,704]{0,1:T(8,128)(2,1)} %param.42, bf16[8,2048]{1,0:T(8,128)(2,1)S(1)} %all_gather.7, f32[2048]{0:T(1024)S(1)} %copy-done.3, f32[8,704]{1,0:T(8,128)S(1)} %convolution_multiply_fusion.1, f32[8]{0:T(128)S(1)} %add_rsqrt_fusion), kind=kOutput, calls=%fused_computation | convolution fusion | flops 46225920 | bytes 5896224 | tf_op jit(solution)/shard_map/dot_general | solution.py:144
  108.3 31.5 %reduce-scatter.5.cloned.1.call-done = f32[256,8]{0,1:T(8,128)} async-done(((f32[2048,8]{0,1:T(8,128)}), f32[256,8]{0,1:T(8,128)}) %reduce-scatter.5.cloned.1.call-update) | async-done | bytes 8208 | tf_op jit(solution)/shard_map/reduce_scatter | solution.py:143
  139.8 1.3 fusion.20
  (40 shorter events, 6.7 us)
Async XLA Ops:
  6.5 97.6 %copy-start = (bf16[704,2048]{1,0:T(8,128)(2,1)S(1)}, bf16[704,2048]{1,0:T(8,128)(2,1)}, u32[]{:S(2)}) copy-start(bf16[704,2048]{1,0:T(8,128)(2,1)} %param.43) | copy-start | bytes 8650756
  6.5 73.4 %copy-start.2 = (bf16[8,512]{1,0:T(8,128)(2,1)S(1)}, bf16[8,512]{1,0:T(8,128)(2,1)}, u32[]{:S(2)}) copy-start(bf16[8,512]{1,0:T(8,128)(2,1)} %param.22) | copy-start | bytes 24580
  6.5 72.6 %copy-start.1 = (bf16[512,512]{1,0:T(8,128)(2,1)S(1)}, bf16[512,512]{1,0:T(8,128)(2,1)}, u32[]{:S(2)}) copy-start(bf16[512,512]{1,0:T(8,128)(2,1)} %param.39) | copy-start | bytes 1572868
  6.5 94.9 %copy-start.3 = (f32[2048]{0:T(1024)S(1)}, f32[2048]{0:T(1024)}, u32[]{:S(2)}) copy-start(f32[2048]{0:T(1024)} %param.40) | copy-start | bytes 24580
  6.5 49.8 %all-reduce.8.cloned.1.call-start = ((), (), s32[]{:S(2)}) async-start(), calls=%async_computation.4 | async-start | bytes 140288
  18.6 67.8 %reduce-scatter.3.cloned.1.call-start = ((), (), s32[]{:S(2)}) async-start(), calls=%async_computation.2 | async-start | bytes 12288 | tf_op jit(solution)/shard_map/reduce_scatter | solution.py:128
  19.3 0.7 copy-start.4
  79.9 59.9 %reduce-scatter.5.cloned.1.call-start = ((), (), s32[]{:S(2)}) async-start(), calls=%async_computation.3 | async-start | bytes 73728 | tf_op jit(solution)/shard_map/reduce_scatter | solution.py:143
Sparse Core Ops, SparseCore 0:
  18.7 37.6 all-reduce.7
  80.0 6.2 reduce-scatter.2
  108.4 31.2 reduce-scatter.4
where the time goes:
time: 149 us; the launch traced here: 148 us
  waiting for transfers between devices  71.9 us (48%)
  blocking collectives  26.3 us (18%)
  matrix products  20.6 us (14%)
  between operations  13.8 us (9%)
  other arithmetic  11.7 us (8%)
  local copies, waits for them, and re-layouts  3.11 us (2%)
    unnamed x4, waiting for transfers between devices  34.1 us
    reduce_scatter x1, waiting for transfers between devices, per_device(): lax.psum_scatter(lax.dot_general(down_weight, hidden_units, (((0,), (1,))...  31.5 us
    all_gather x1, blocking collectives, per_device(): lax.all_gather(residual, ('kv', 'tp'), axis=1, tiled=True)  14.3 us
    all_gather x1, blocking collectives, per_device(): lax.all_gather(mixed_heads, 'kv', axis=0, tiled=True)  12 us
    dot_general x5, matrix products, product(): return jnp.dot(normed, weight, preferred_element_type=jnp.float32)  8.84 us
    reduce_scatter x1, waiting for transfers between devices, per_device(): lax.psum_scatter(mix_terms.astype(jnp.bfloat16), 'tp', scatter_dimension=...  6.35 us
    dot_general x1, matrix products, per_device(): lax.dot_general(down_weight, hidden_units, (((0,), (1,)), ((), ())), pref...  4.12 us
  transfers between devices with their start and end apart: 3, of which 3 were waited for; matrix products, arithmetic and copies ran while one was open for 2% of the time, Pallas kernels for 0%

commit v1 on v0

--- a/solution.py
+++ b/solution.py
@@ -4,6 +4,18 @@
 from jax.sharding import PartitionSpec as P
 
 EPS = 1e-06
+
+
+def collect(array, axis, dim):
+    ways, here, step = (lax.axis_size(axis), lax.axis_index(axis), array.shape[dim])
+    dims = [n * ways if d == dim else n for d, n in enumerate(array.shape)]
+    full = lax.dynamic_update_slice_in_dim(
+        jnp.zeros(dims, array.dtype), array, here * step, axis=dim
+    )
+    for far in range(1, ways):
+        array = lax.ppermute(array, axis, [(d, (d + 1) % ways) for d in range(ways)])
+        full = lax.dynamic_update_slice_in_dim(full, array, (here - far) % ways * step, axis=dim)
+    return full
 
 
 def per_device(
@@ -132,7 +144,7 @@
     residual = (
         lax.dynamic_slice_in_dim(token_values, half_index * narrow, narrow, 1) + mix_sum
     ).astype(jnp.bfloat16)
-    piece_wide = lax.all_gather(residual, ("kv", "tp"), axis=1, tiled=True).astype(jnp.float32)
+    piece_wide = collect(residual, ("kv", "tp"), 1).astype(jnp.float32)
     normed_piece = (piece_wide * mixer_gain[None, :]).astype(jnp.bfloat16)
     gate_acc = jnp.dot(normed_piece, gate_weight, preferred_element_type=jnp.float32)
     up_acc = jnp.dot(normed_piece, up_weight, preferred_element_type=jnp.float32)

time: 149 us -> 166 us (1.11)
  waiting for transfers between devices: 71.9 us -> 103 us
  blocking collectives: 26.3 us -> 12 us
    ppermute x0 -> x7, waiting for transfers between devices: none -> 33.6 us  [collect(): lax.ppermute(array, axis, [(d, (d + 1) % ways) for d in range(ways)])]
    all_gather x1 -> x0, blocking collectives: 14.3 us -> none  [per_device(): lax.all_gather(residual, ('kv', 'tp'), axis=1, tiled=True)]
    reduce_scatter x1, waiting for transfers between devices: 31.5 us -> 29 us  [per_device(): lax.psum_scatter(lax.dot_general(down_weight, hidden_units, (((0,), (1,))...]
  transfers between devices with their start and end apart: 3 -> 10, of which waited for: 3 -> 10; matrix products, arithmetic and copies ran while one was open for 2% -> 2% of each run, Pallas kernels for 0% -> 0%
where the time goes in v1:
time: 166 us; the launch traced here: 165 us
  waiting for transfers between devices  103 us (62%)
  matrix products  20.6 us (12%)
  between operations  13.9 us (8%)
  blocking collectives  12 us (7%)
  other arithmetic  11.7 us (7%)
  local copies, waits for them, and re-layouts  3.13 us (2%)
    unnamed x4, waiting for transfers between devices  34.1 us
    ppermute x7, waiting for transfers between devices, collect(): lax.ppermute(array, axis, [(d, (d + 1) % ways) for d in range(ways)])  33.6 us
    reduce_scatter x1, waiting for transfers between devices, per_device(): lax.psum_scatter(lax.dot_general(down_weight, hidden_units, (((0,), (1,))...  29 us
    all_gather x1, blocking collectives, per_device(): lax.all_gather(mixed_heads, 'kv', axis=0, tiled=True)  12 us
    dot_general x5, matrix products, product(): return jnp.dot(normed, weight, preferred_element_type=jnp.float32)  8.84 us
    reduce_scatter x1, waiting for transfers between devices, per_device(): lax.psum_scatter(mix_terms.astype(jnp.bfloat16), 'tp', scatter_dimension=...  6.3 us
    dot_general x1, matrix products, per_device(): lax.dot_general(down_weight, hidden_units, (((0,), (1,)), ((), ())), pref...  4.12 us
  transfers between devices with their start and end apart: 10, of which 10 were waited for; matrix products, arithmetic and copies ran while one was open for 2% of the time, Pallas kernels for 0%

profile of v1, /device:TPU:0, one launch (start us, length us, event | category | flops | bytes accessed | tf_op | source)
XLA Modules:
  0.0 164.6 jit_solution(7517385458960251174)
XLA Ops:
  6.6 1.6 multiply_reduce_fusion
  8.2 1.9 %fusion.43 = f32[8,512]{1,0:T(8,128)} fusion(bf16[512,512]{1,0:T(8,128)(2,1)} %param.27, f32[512]{0:T(512)} %param.23, bf16[8,512]{1,0:T(8,128)(2,1)} %param.22), kind=kOutput, calls=%fused_computation.81 | convolution fusion | flops 4206592 | bytes 550912 | tf_op jit(solution)/shard_map/dot_general | solution.py:67
  10.0 1.9 %fusion.44 = f32[8,512]{1,0:T(8,128)} fusion(bf16[512,512]{1,0:T(8,128)(2,1)} %param.26, f32[512]{0:T(512)} %param.23, bf16[8,512]{1,0:T(8,128)(2,1)} %param.22), kind=kOutput, calls=%fused_computation.82 | convolution fusion | flops 4206592 | bytes 550912 | tf_op jit(solution)/shard_map/dot_general | solution.py:67
  11.9 1.9 %fusion.46 = f32[8,512]{1,0:T(8,128)} fusion(bf16[512,512]{1,0:T(8,128)(2,1)} %param.24, f32[512]{0:T(512)} %param.23, bf16[8,512]{1,0:T(8,128)(2,1)} %param.22), kind=kOutput, calls=%fused_computation.84 | convolution fusion | flops 4206592 | bytes 550912 | tf_op jit(solution)/shard_map/dot_general | solution.py:67
  15.3 1.9 %fusion.45 = f32[8,512]{1,0:T(8,128)} fusion(bf16[512,512]{1,0:T(8,128)(2,1)} %param.25, f32[512]{0:T(512)} %param.23, bf16[8,512]{1,0:T(8,128)(2,1)} %param.22), kind=kOutput, calls=%fused_computation.83 | convolution fusion | flops 4206592 | bytes 550912 | tf_op jit(solution)/shard_map/dot_general | solution.py:67
  17.1 1.4 fusion.21
  20.3 1.3 dynamic-slice
  22.3 34.1 %all-reduce.8.cloned.1.call-done = (f32[8,512]{1,0:T(8,128)}, f32[8]{0:T(128)}, f32[8,512]{1,0:T(8,128)}, f32[8,512]{1,0:T(8,128)}, f32[8,4]{1,0:T(8,128)}, /*index=5*/f32[8,512]{1,0:T(8,128)}) async-done(((f32[8,512]{1,0:T(8,128)}, f32[8]{0:T(128)}, f32[8,512]{1,0:T(8,128)}, f32[8,512]{1,0:T(8,128)}, f32[8,4]{1,0:T(8,128)}, /*index=5*/f32[8,512]{1,0:T(8,128)}), (f32[8,512]{1,0:T(8,128)}, f32[8]{0:T(128)}, ...) | async-done | bytes 65712
  58.7 1.0 fusion.5
  62.2 1.0 fusion.2
  64.0 2.2 %fusion.31 = f32[2,2,1,256]{3,2,1,0:T(1,128)S(1)} fusion(f32[2,2,256,256]{3,2,1,0:T(8,128)} %param.35, f32[2,2,256,1]{2,1,0,3:T(2,128)S(1)} %get-tuple-element.22), kind=kOutput, calls=%fused_computation.46 | convolution fusion | flops 3145728 | bytes 1056768 | tf_op jit(solution)/shard_map/shvd,shd->shv/dot_general | solution.py:117
  67.1 12.0 %all-gather = bf16[4,2,512]{2,1,0:T(2,128)(2,1)S(1)} all-gather(bf16[1,2,512]{2,1,0:T(2,128)(2,1)S(1)} %fusion.39), channel_id=1, replica_groups=mesh['dp'=4,'kv'=4,'tp'=2] {'kv'}, dimensions={0}, use_global_device_ids=true | all-gather | bytes 10240 | tf_op jit(solution)/shard_map/all_gather | solution.py:136
  80.0 6.3 %reduce-scatter.3.cloned.1.call-done = bf16[8,256]{1,0:T(8,128)(2,1)} async-done(((bf16[8,512]{1,0:T(8,128)(2,1)}), bf16[8,256]{1,0:T(8,128)(2,1)}) %reduce-scatter.3.cloned.1.call-update) | async-done | bytes 4112 | tf_op jit(solution)/shard_map/reduce_scatter | solution.py:140
  87.2 4.6 %collective-permute-done = bf16[8,256]{1,0:T(8,128)(2,1)S(1)} collective-permute-done((bf16[8,256]{1,0:T(8,128)(2,1)S(1)}, bf16[8,256]{1,0:T(8,128)(2,1)S(1)}, u32[]{:S(2)}, u32[]{:S(2)}) %collective-permute-start) | collective-permute-done | bytes 4128 | tf_op jit(solution)/shard_map/ppermute | solution.py:16
  91.9 4.8 %collective-permute-done.1 = bf16[8,256]{1,0:T(8,128)(2,1)S(1)} collective-permute-done((bf16[8,256]{1,0:T(8,128)(2,1)S(1)}, bf16[8,256]{1,0:T(8,128)(2,1)S(1)}, u32[]{:S(2)}, u32[]{:S(2)}) %collective-permute-start.1) | collective-permute-done | bytes 4128 | tf_op jit(solution)/shard_map/ppermute | solution.py:16
  96.7 4.8 %collective-permute-done.2 = bf16[8,256]{1,0:T(8,128)(2,1)S(1)} collective-permute-done((bf16[8,256]{1,0:T(8,128)(2,1)S(1)}, bf16[8,256]{1,0:T(8,128)(2,1)S(1)}, u32[]{:S(2)}, u32[]{:S(2)}) %collective-permute-start.2) | collective-permute-done | bytes 4128 | tf_op jit(solution)/shard_map/ppermute | solution.py:16
  101.5 4.8 %collective-permute-done.3 = bf16[8,256]{1,0:T(8,128)(2,1)S(1)} collective-permute-done((bf16[8,256]{1,0:T(8,128)(2,1)S(1)}, bf16[8,256]{1,0:T(8,128)(2,1)S(1)}, u32[]{:S(2)}, u32[]{:S(2)}) %collective-permute-start.3) | collective-permute-done | bytes 4128 | tf_op jit(solution)/shard_map/ppermute | solution.py:16
  106.3 4.8 %collective-permute-done.4 = bf16[8,256]{1,0:T(8,128)(2,1)S(1)} collective-permute-done((bf16[8,256]{1,0:T(8,128)(2,1)S(1)}, bf16[8,256]{1,0:T(8,128)(2,1)S(1)}, u32[]{:S(2)}, u32[]{:S(2)}) %collective-permute-start.4) | collective-permute-done | bytes 4128 | tf_op jit(solution)/shard_map/ppermute | solution.py:16
  111.2 4.8 %collective-permute-done.5 = bf16[8,256]{1,0:T(8,128)(2,1)S(1)} collective-permute-done((bf16[8,256]{1,0:T(8,128)(2,1)S(1)}, bf16[8,256]{1,0:T(8,128)(2,1)S(1)}, u32[]{:S(2)}, u32[]{:S(2)}) %collective-permute-start.5) | collective-permute-done | bytes 4128 | tf_op jit(solution)/shard_map/ppermute | solution.py:16
  116.0 4.8 %collective-permute-done.6 = bf16[8,256]{1,0:T(8,128)(2,1)S(1)} collective-permute-done((bf16[8,256]{1,0:T(8,128)(2,1)S(1)}, bf16[8,256]{1,0:T(8,128)(2,1)S(1)}, u32[]{:S(2)}, u32[]{:S(2)}) %collective-permute-start.6) | collective-permute-done | bytes 4128 | tf_op jit(solution)/shard_map/ppermute | solution.py:16
  121.0 2.7 %convolution_multiply_fusion.1 = f32[8,704]{1,0:T(8,128)S(1)} fusion(bf16[2048,704]{0,1:T(8,128)(2,1)} %param.41, bf16[8,2048]{1,0:T(8,128)(2,1)S(1)} %constant_dynamic-update-slice_fusion, f32[2048]{0:T(1024)S(1)} %copy-done.3, f32[8]{0:T(128)S(1)} %add_rsqrt_fusion), kind=kOutput, calls=%fused_computation.3 | convolution fusion | flops 23123456 | bytes 2947104 | tf_op jit(solution)/shard_map/dot_general | solution.py:149
  123.6 4.1 %convolution_bitcast_fusion = f32[2048,8]{0,1:T(8,128)} fusion(bf16[704,2048]{1,0:T(8,128)(2,1)S(1)} %copy-done, bf16[2048,704]{0,1:T(8,128)(2,1)} %param.42, bf16[8,2048]{1,0:T(8,128)(2,1)S(1)} %constant_dynamic-update-slice_fusion, f32[2048]{0:T(1024)S(1)} %copy-done.3, f32[8,704]{1,0:T(8,128)S(1)} %convolution_multiply_fusion.1, f32[8]{0:T(128)S(1)} %add_rsqrt_fusion), kind=kOutput, calls=%fused_computation | convolution fusion | flops 46225920 | bytes 5896224 | tf_op jit(solution)/shard_map/dot_general | solution.py:156
  127.8 29.0 %reduce-scatter.5.cloned.1.call-done = f32[256,8]{0,1:T(8,128)} async-done(((f32[2048,8]{0,1:T(8,128)}), f32[256,8]{0,1:T(8,128)}) %reduce-scatter.5.cloned.1.call-update) | async-done | bytes 8208 | tf_op jit(solution)/shard_map/reduce_scatter | solution.py:155
  156.8 1.3 fusion.20
  (61 shorter events, 11.8 us)
Async XLA Ops:
  6.5 117.1 %copy-start = (bf16[704,2048]{1,0:T(8,128)(2,1)S(1)}, bf16[704,2048]{1,0:T(8,128)(2,1)}, u32[]{:S(2)}) copy-start(bf16[704,2048]{1,0:T(8,128)(2,1)} %param.43) | copy-start | bytes 8650756
  6.5 73.4 %copy-start.2 = (bf16[8,512]{1,0:T(8,128)(2,1)S(1)}, bf16[8,512]{1,0:T(8,128)(2,1)}, u32[]{:S(2)}) copy-start(bf16[8,512]{1,0:T(8,128)(2,1)} %param.22) | copy-start | bytes 24580
  6.5 72.6 %copy-start.1 = (bf16[512,512]{1,0:T(8,128)(2,1)S(1)}, bf16[512,512]{1,0:T(8,128)(2,1)}, u32[]{:S(2)}) copy-start(bf16[512,512]{1,0:T(8,128)(2,1)} %param.39) | copy-start | bytes 1572868
  6.5 114.4 %copy-start.3 = (f32[2048]{0:T(1024)S(1)}, f32[2048]{0:T(1024)}, u32[]{:S(2)}) copy-start(f32[2048]{0:T(1024)} %param.40) | copy-start | bytes 24580
  6.5 49.8 %all-reduce.8.cloned.1.call-start = ((), (), s32[]{:S(2)}) async-start(), calls=%async_computation.4 | async-start | bytes 140288
  18.6 67.8 %reduce-scatter.3.cloned.1.call-start = ((), (), s32[]{:S(2)}) async-start(), calls=%async_computation.2 | async-start | bytes 12288 | tf_op jit(solution)/shard_map/reduce_scatter | solution.py:140
  19.3 0.7 copy-start.4
  79.9 76.9 %reduce-scatter.5.cloned.1.call-start = ((), (), s32[]{:S(2)}) async-start(), calls=%async_computation.3 | async-start | bytes 73728 | tf_op jit(solution)/shard_map/reduce_scatter | solution.py:155
  87.0 4.8 %collective-permute-start = (bf16[8,256]{1,0:T(8,128)(2,1)S(1)}, bf16[8,256]{1,0:T(8,128)(2,1)S(1)}, u32[]{:S(2)}, u32[]{:S(2)}) collective-permute-start(bf16[8,256]{1,0:T(8,128)(2,1)S(1)} %get-tuple-element.14), channel_id=1, source_target_pairs={{0,1},{1,2},{2,3},{3,4},{4,5},{5,6},{6,7},{7,0},{8,9},{9,10},{10,1... | collective-permute-start | bytes 12296 | tf_op jit(solution)/shard_map/ppermute | solution.py:16
  91.8 4.8 %collective-permute-start.1 = (bf16[8,256]{1,0:T(8,128)(2,1)S(1)}, bf16[8,256]{1,0:T(8,128)(2,1)S(1)}, u32[]{:S(2)}, u32[]{:S(2)}) collective-permute-start(bf16[8,256]{1,0:T(8,128)(2,1)S(1)} %collective-permute-done), channel_id=1, source_target_pairs={{0,1},{1,2},{2,3},{3,4},{4,5},{5,6},{6,7},{7,0},{8,9},{9,10},{10,1... | collective-permute-start | bytes 12296 | tf_op jit(solution)/shard_map/ppermute | solution.py:16
  96.7 4.8 %collective-permute-start.2 = (bf16[8,256]{1,0:T(8,128)(2,1)S(1)}, bf16[8,256]{1,0:T(8,128)(2,1)S(1)}, u32[]{:S(2)}, u32[]{:S(2)}) collective-permute-start(bf16[8,256]{1,0:T(8,128)(2,1)S(1)} %collective-permute-done.1), channel_id=1, source_target_pairs={{0,1},{1,2},{2,3},{3,4},{4,5},{5,6},{6,7},{7,0},{8,9},{9,10},{10,1... | collective-permute-start | bytes 12296 | tf_op jit(solution)/shard_map/ppermute | solution.py:16
  101.5 4.8 %collective-permute-start.3 = (bf16[8,256]{1,0:T(8,128)(2,1)S(1)}, bf16[8,256]{1,0:T(8,128)(2,1)S(1)}, u32[]{:S(2)}, u32[]{:S(2)}) collective-permute-start(bf16[8,256]{1,0:T(8,128)(2,1)S(1)} %collective-permute-done.2), channel_id=1, source_target_pairs={{0,1},{1,2},{2,3},{3,4},{4,5},{5,6},{6,7},{7,0},{8,9},{9,10},{10,1... | collective-permute-start | bytes 12296 | tf_op jit(solution)/shard_map/ppermute | solution.py:16
  106.3 4.8 %collective-permute-start.4 = (bf16[8,256]{1,0:T(8,128)(2,1)S(1)}, bf16[8,256]{1,0:T(8,128)(2,1)S(1)}, u32[]{:S(2)}, u32[]{:S(2)}) collective-permute-start(bf16[8,256]{1,0:T(8,128)(2,1)S(1)} %collective-permute-done.3), channel_id=1, source_target_pairs={{0,1},{1,2},{2,3},{3,4},{4,5},{5,6},{6,7},{7,0},{8,9},{9,10},{10,1... | collective-permute-start | bytes 12296 | tf_op jit(solution)/shard_map/ppermute | solution.py:16
  111.2 4.8 %collective-permute-start.5 = (bf16[8,256]{1,0:T(8,128)(2,1)S(1)}, bf16[8,256]{1,0:T(8,128)(2,1)S(1)}, u32[]{:S(2)}, u32[]{:S(2)}) collective-permute-start(bf16[8,256]{1,0:T(8,128)(2,1)S(1)} %collective-permute-done.4), channel_id=1, source_target_pairs={{0,1},{1,2},{2,3},{3,4},{4,5},{5,6},{6,7},{7,0},{8,9},{9,10},{10,1... | collective-permute-start | bytes 12296 | tf_op jit(solution)/shard_map/ppermute | solution.py:16
  116.0 4.8 %collective-permute-start.6 = (bf16[8,256]{1,0:T(8,128)(2,1)S(1)}, bf16[8,256]{1,0:T(8,128)(2,1)S(1)}, u32[]{:S(2)}, u32[]{:S(2)}) collective-permute-start(bf16[8,256]{1,0:T(8,128)(2,1)S(1)} %collective-permute-done.5), channel_id=1, source_target_pairs={{0,1},{1,2},{2,3},{3,4},{4,5},{5,6},{6,7},{7,0},{8,9},{9,10},{10,1... | collective-permute-start | bytes 12296 | tf_op jit(solution)/shard_map/ppermute | solution.py:16
Sparse Core Ops, SparseCore 0:
  18.7 37.6 all-reduce.7
  80.0 6.2 reduce-scatter.2
  127.9 28.8 reduce-scatter.4
